TPU v7x, 32 devices: a whole 2x2x4 slice. The times are simulated.
32 devices in a mesh: grp: 2 (over x), ep: 8 (over z, y), tp: 2 (over core).
Axes of the slice: x: 2, y: 2, z: 4, core: 2. Of those that a mesh axis runs over, the one named last changes fastest.
Arguments:
- tokens: bfloat16 [8192, 2048], P(('grp', 'ep', 'tp')), parts along dimension 0, may hold values from -6 to 6
- norm_gain: float32 [2048], replicated, may hold values from 0.1 to 1.9
- expert_ids: int32 [8192, 4], P(('grp', 'ep', 'tp')), parts along dimension 0, may hold values from 0 to 31, all different within a row; in each aligned block of 256 rows (0 to 255, 256 to 511, ...) at most 40 rows name the same one
- gate_weights: float32 [8192, 4], P(('grp', 'ep', 'tp')), parts along dimension 0, may hold values from 0.1 to 1
- expert_gate: bfloat16 [32, 2048, 512], P('ep', None, 'tp'), may hold values from -0.125 to 0.125
- expert_up: bfloat16 [32, 2048, 512], P('ep', None, 'tp'), may hold values from -0.125 to 0.125
- expert_down: bfloat16 [32, 512, 2048], P('ep', 'tp'), may hold values from -0.25 to 0.25
- shared_gate: bfloat16 [2048, 512], replicated, may hold values from -0.125 to 0.125
- shared_up: bfloat16 [2048, 512], replicated, may hold values from -0.125 to 0.125
- shared_down: bfloat16 [512, 2048], replicated, may hold values from -0.25 to 0.25
- post_gain: float32 [2048], replicated, may hold values from 0.1 to 1.9
Outputs:
- mixed: bfloat16 [8192, 2048], P(('grp', 'ep', 'tp')), parts along dimension 0
There are 2 independent parts, one for each index of `grp`. A program takes and returns all parts, laid end to end along the dimension named above; an argument that names none is the same for every part. Nothing has to cross between parts.
Inputs may be any that keep to these rules, and one draw needn't show every extreme that they name: `expert_ids`: each row names 4 different experts; in each device's aligned block of 256 rows no expert is named by more than 40 rows, a bound that some block reaches.
All inputs are finite; a program needn't handle non-finite values.
Results may differ from a plain program's by a relative error of at most 0.0067.
Values may be sent and summed in bfloat16 or wider, within the bound.
A program may use at most 128 MiB of HBM per device.

v0:
```python
import jax
import jax.numpy as jnp
from jax import lax
from jax.sharding import PartitionSpec as P

EXPERTS = 32
CAP = 40


EPS = 1e-06


def rms_scale(inputs, gain):
    mean_sq = jnp.mean(inputs * inputs, axis=-1, keepdims=True)
    return inputs * lax.rsqrt(mean_sq + EPS) * gain


def expert_rows(tok_rows, w_gate, w_up, w_down):
    gate_act = jnp.einsum("erd,edf->erf", tok_rows, w_gate, preferred_element_type=jnp.float32)
    up_act = jnp.einsum("erd,edf->erf", tok_rows, w_up, preferred_element_type=jnp.float32)
    hidden = (jax.nn.silu(gate_act) * up_act).astype(jnp.bfloat16)
    return jnp.einsum("erf,efd->erd", hidden, w_down, preferred_element_type=jnp.float32)


def shared_branch(normed, shared_gate, shared_up, shared_down):
    shared_act = jnp.dot(normed, shared_gate, preferred_element_type=jnp.float32)
    shared_lift = jnp.dot(normed, shared_up, preferred_element_type=jnp.float32)
    shared_hidden = (jax.nn.silu(shared_act) * shared_lift).astype(jnp.bfloat16)
    return jnp.dot(shared_hidden, shared_down, preferred_element_type=jnp.float32)


def body(
    tokens,
    norm_gain,
    expert_ids,
    gate_weights,
    expert_gate,
    expert_up,
    expert_down,
    shared_gate,
    shared_up,
    shared_down,
    post_gain,
):
    tok_count = tokens.shape[0]
    top_count = expert_ids.shape[1]
    width = tokens.shape[1]
    normed = rms_scale(tokens.astype(jnp.float32), norm_gain).astype(jnp.bfloat16)
    flat_ids = expert_ids.reshape(-1)
    onehot = (flat_ids[:, None] == jnp.arange(EXPERTS, dtype=jnp.int32)[None, :]).astype(jnp.int32)
    slot_index = jnp.sum(jnp.cumsum(onehot, axis=0) * onehot, axis=1) - 1
    position = flat_ids * CAP + slot_index
    source_row = jnp.arange(tok_count * top_count, dtype=jnp.int32) // top_count
    lookup = jnp.full((EXPERTS * CAP,), tok_count, jnp.int32).at[position].set(source_row)
    padded = jnp.concatenate([normed, jnp.zeros((1, width), jnp.bfloat16)], axis=0)
    outgoing = padded[lookup].reshape(EXPERTS, 1, CAP, width)
    whole_gate, whole_up, whole_down = (
        lax.all_gather(expert_gate, "tp", axis=2, tiled=True),
        lax.all_gather(expert_up, "tp", axis=2, tiled=True),
        lax.all_gather(expert_down, "tp", axis=1, tiled=True),
    )
    arrived = lax.all_to_all(outgoing, "ep", split_axis=0, concat_axis=1, tiled=True)
    local_experts = arrived.shape[0]
    senders = arrived.shape[1]
    slots = arrived.shape[2]
    tok_rows = arrived.reshape(local_experts, senders * slots, width)
    result = expert_rows(tok_rows, whole_gate, whole_up, whole_down).astype(jnp.bfloat16)
    result = result.reshape(local_experts, senders, slots, width)
    returned = lax.all_to_all(result, "ep", split_axis=1, concat_axis=0, tiled=True)
    shared_out = shared_branch(normed, shared_gate, shared_up, shared_down)
    back_rows = returned.reshape(EXPERTS * CAP, width)
    picked = back_rows[position].reshape(tok_count, top_count, width).astype(jnp.float32)
    routed = jnp.einsum("tk,tkd->td", gate_weights, picked)
    combined = routed + shared_out
    return rms_scale(combined, post_gain).astype(jnp.bfloat16)


def solution(mesh):
    return jax.shard_map(
        body,
        mesh=mesh,
        in_specs=(
            P(("grp", "ep", "tp"), None),
            P(),
            P(("grp", "ep", "tp"), None),
            P(("grp", "ep", "tp"), None),
            P("ep", None, "tp"),
            P("ep", None, "tp"),
            P("ep", "tp", None),
            P(),
            P(),
            P(),
            P(),
        ),
        out_specs=P(("grp", "ep", "tp"), None),
        check_vma=False,
    )
```

profile of v0, /device:TPU:0, one launch (start us, length us, event | category | flops | bytes accessed | tf_op | source)
XLA Modules:
  0.0 349.9 jit_solution(3628326281453498933)
XLA Ops:
  6.5 0.7 all-gather.4.cloned.1.call-update
  7.3 0.7 all-gather.6.cloned.1.call-update
  8.4 9.0 %reduce-window.6 = s32[32,8,128]{2,1,0:T(8,128)S(1)} reduce-window(s32[32,8,128]{2,1,0:T(8,128)S(1)} %fusion.12, s32[]{:T(128)} %constant.42.clone.1), window={size=1x1x128 pad=0_0x0_0x127_0}, to_apply=%region_1.0 | reduce-window | flops 4161536 | bytes 262148 | tf_op jit(solution)/shard_map/reduce-window
  18.1 0.3 fusion
  18.4 0.3 fusion.2
  18.7 1.0 copy-done.2
  20.0 4.3 %scatter_custom_fusion = s32[1280]{0:T(1024)S(1)} fusion(s32[1024]{0:T(1024)S(1)} %bitcast.59, s32[1024]{0:T(1024)S(1)} %add_select_fusion, s32[]{:T(128)} %constant.40.clone.1), kind=kCustom, calls=%fused_computation.37 | custom fusion | bytes 5124 | tf_op jit(solution)/shard_map/scatter | solution.py:54
  24.3 6.2 %gather_fusion = bf16[1280,2048]{1,0:T(8,128)(2,1)} fusion(bf16[257,2048]{1,0:T(8,128)(2,1)S(1)} %concatenate.3, s32[2048]{0:T(1024)S(1)} %pad_clamp_fusion), kind=kCustom, calls=%fused_computation | custom fusion | bytes 10490880 | tf_op jit(solution)/shard_map/gather | solution.py:56
  30.5 7.3 %all-to-all-start = ((bf16[32,1,40,2048]{3,2,1,0:T(8,128)(2,1)}), bf16[32,1,40,2048]{3,2,1,0:T(8,128)(2,1)}, u32[]{:S(2)}, u32[]{:S(2)}) async-start(bf16[32,1,40,2048]{3,2,1,0:T(8,128)(2,1)} %bitcast.53), calls=%async_computation | async-start | bytes 10485760 | tf_op jit(solution)/shard_map/all_to_all | solution.py:62
  37.9 0.7 all-gather.8.cloned.1.call-update
  38.6 115.0 %all-to-all-done = bf16[32,1,40,2048]{3,2,1,0:T(8,128)(2,1)} async-done(((bf16[32,1,40,2048]{3,2,1,0:T(8,128)(2,1)}), bf16[32,1,40,2048]{3,2,1,0:T(8,128)(2,1)}, u32[]{:S(2)}, u32[]{:S(2)}) %all-to-all-start) | async-done | bytes 5242912 | tf_op jit(solution)/shard_map/all_to_all | solution.py:62
  153.6 5.7 %copy.26 = bf16[4,8,1,40,2048]{4,3,1,0,2:T(8,128)(2,1)} copy(bf16[4,8,1,40,2048]{4,3,0,1,2:T(8,128)(2,1)} %bitcast.7) | data formatting | bytes 10485760 | tf_op jit(solution)/shard_map/all_to_all | solution.py:62
  159.3 9.3 %fusion.19 = f32[4,320,512]{2,1,0:T(8,128)} fusion(bf16[4,320,2048]{2,1,0:T(8,128)(2,1)} %bitcast.54, bf16[4,2048,512]{2,1,0:T(8,128)(2,1)} %all-gather.4.cloned.1.call-done), kind=kOutput, calls=%fused_computation.46 | convolution fusion | flops 2684354560 | bytes 16252928 | tf_op jit(solution)/shard_map/erd,edf->erf/dot_general | solution.py:19
  168.6 16.2 %convolution_convert_fusion = bf16[4,320,2048]{2,1,0:T(8,128)(2,1)} fusion(bf16[4,512,2048]{2,1,0:T(8,128)(2,1)} %all-gather.8.cloned.1.call-done, f32[4,320,512]{2,1,0:T(8,128)} %fusion.19, bf16[4,320,2048]{2,1,0:T(8,128)(2,1)} %bitcast.55, bf16[4,2048,512]{2,1,0:T(8,128)(2,1)} %all-gather.6.cloned.1.call-done), kind=kOutput, calls=%fused_computation.3 | convolution fusion | flops 5375262720 | bytes 29884416 | tf_op jit(solution)/shard_map/erf,efd->erd/dot_general | solution.py:22
  184.8 5.6 %copy.27 = bf16[4,8,40,2048]{3,2,0,1:T(8,128)(2,1)} copy(bf16[4,8,40,2048]{3,2,1,0:T(8,128)(2,1)} %bitcast.56) | data formatting | bytes 10485760 | tf_op jit(solution)/shard_map/reshape | solution.py:68
  190.4 5.0 %all-to-all-start.1 = ((bf16[4,8,40,2048]{3,2,0,1:T(8,128)(2,1)}), bf16[4,8,40,2048]{3,2,0,1:T(8,128)(2,1)}, u32[]{:S(2)}, u32[]{:S(2)}) async-start(bf16[4,8,40,2048]{3,2,0,1:T(8,128)(2,1)} %copy.27), calls=%async_computation.1 | async-start | bytes 10485760 | tf_op jit(solution)/shard_map/all_to_all | solution.py:69
  195.4 0.2 copy.28
  195.6 3.1 fusion.21
  198.7 111.4 %all-to-all-done.1 = bf16[4,8,40,2048]{3,2,0,1:T(8,128)(2,1)} async-done(((bf16[4,8,40,2048]{3,2,0,1:T(8,128)(2,1)}), bf16[4,8,40,2048]{3,2,0,1:T(8,128)(2,1)}, u32[]{:S(2)}, u32[]{:S(2)}) %all-to-all-start.1) | async-done | bytes 5242912 | tf_op jit(solution)/shard_map/all_to_all | solution.py:69
  310.1 12.0 %gather_fusion.1 = bf16[1024,2048]{1,0:T(8,128)(2,1)} fusion(bf16[1280,2048]{1,0:T(8,128)(2,1)} %bitcast.12, s32[1024]{0:T(1024)S(1)} %broadcast_clamp_fusion), kind=kCustom, calls=%fused_computation.1 | custom fusion | bytes 8392704 | tf_op jit(solution)/shard_map/gather | solution.py:72
  322.1 7.2 %reshape.91 = bf16[256,4,2048]{2,1,0:T(4,128)(2,1)} reshape(bf16[1024,2048]{1,0:T(8,128)(2,1)} %gather_fusion.1) | data formatting | bytes 8388608 | tf_op jit(solution)/shard_map/reshape | solution.py:72
  329.3 5.8 %fusion.20 = f32[256,1,2048]{2,1,0:T(1,128)} fusion(bf16[256,4,2048]{2,1,0:T(4,128)(2,1)} %reshape.91, bf16[256,4,1]{1,2,0:T(2,128)(2,1)S(1)} %copy.28), kind=kOutput, calls=%fused_computation.47 | convolution fusion | flops 4194304 | bytes 6293504 | tf_op jit(solution)/shard_map/tk,tkd->td/dot_general | solution.py:73
  335.1 5.5 %multiply_reduce_fusion = (f32[256]{0:T(256)S(1)}, f32[256,2048]{1,0:T(8,128)}) fusion(bf16[512,2048]{1,0:T(8,128)(2,1)S(1)} %copy-done, bf16[256,2048]{1,0:T(8,128)(2,1)S(1)} %copy-done.3, bf16[2048,512]{1,0:T(8,128)(2,1)} %param.19, f32[256,512]{1,0:T(8,128)} %fusion.21, f32[256,1,2048]{2,1,0:T(1,128)} %fusion.20), kind=kOutput, calls=%fused_computation.12 | convolution fusion | flops 1076100864 | bytes 9962496 | tf_op jit(solution)/shard_map/dot_general | solution.py:29
  340.6 2.8 multiply_convert_fusion.1
  (44 shorter events, 1.4 us)
Async XLA Ops:
  6.5 328.6 %copy-start = (bf16[512,2048]{1,0:T(8,128)(2,1)S(1)}, bf16[512,2048]{1,0:T(8,128)(2,1)}, u32[]{:S(2)}) copy-start(bf16[512,2048]{1,0:T(8,128)(2,1)} %param.20) | copy-start | bytes 6291460
  6.5 152.8 %all-gather.4.cloned.1.call-start = ((), (), s32[]{:S(2)}) async-start(), calls=%async_computation.2 | async-start | bytes 12582912 | tf_op jit(solution)/shard_map/all_gather | solution.py:58
  7.3 0.8 copy-start.4
  7.3 10.8 %copy-start.1 = (bf16[256,2048]{1,0:T(8,128)(2,1)S(1)}, bf16[256,2048]{1,0:T(8,128)(2,1)}, u32[]{:S(2)}) copy-start(bf16[256,2048]{1,0:T(8,128)(2,1)} %param.11) | copy-start | bytes 3145732
  7.3 11.1 %copy-start.5 = (f32[2048]{0:T(1024)S(1)}, f32[2048]{0:T(1024)}, u32[]{:S(2)}) copy-start(f32[2048]{0:T(1024)} %param.12) | copy-start | bytes 24580
  7.3 161.3 %all-gather.6.cloned.1.call-start = ((), (), s32[]{:S(2)}) async-start(), calls=%async_computation.3 | async-start | bytes 12582912 | tf_op jit(solution)/shard_map/all_gather | solution.py:59
  18.7 1.0 copy-start.2
  30.5 123.1 %all-to-all-start = ((bf16[32,1,40,2048]{3,2,1,0:T(8,128)(2,1)}), bf16[32,1,40,2048]{3,2,1,0:T(8,128)(2,1)}, u32[]{:S(2)}, u32[]{:S(2)}) async-start(bf16[32,1,40,2048]{3,2,1,0:T(8,128)(2,1)} %bitcast.53), calls=%async_computation | async-start | bytes 10485760 | tf_op jit(solution)/shard_map/all_to_all | solution.py:62
  37.8 130.8 %all-gather.8.cloned.1.call-start = ((), (), s32[]{:S(2)}) async-start(), calls=%async_computation.4 | async-start | bytes 12582912 | tf_op jit(solution)/shard_map/all_gather | solution.py:60
  190.4 5.0 %copy-start.7 = (f32[256,4]{0,1:T(4,128)S(1)}, f32[256,4]{0,1:T(4,128)}, u32[]{:S(2)}) copy-start(f32[256,4]{0,1:T(4,128)} %param.14) | copy-start | bytes 12292
  190.4 5.2 %copy-start.3 = (bf16[256,2048]{1,0:T(8,128)(2,1)S(1)}, bf16[256,2048]{1,0:T(8,128)(2,1)}, u32[]{:S(2)}) copy-start(bf16[256,2048]{1,0:T(8,128)(2,1)} %copy-done.2) | copy-start | bytes 3145732
  190.4 119.7 %all-to-all-start.1 = ((bf16[4,8,40,2048]{3,2,0,1:T(8,128)(2,1)}), bf16[4,8,40,2048]{3,2,0,1:T(8,128)(2,1)}, u32[]{:S(2)}, u32[]{:S(2)}) async-start(bf16[4,8,40,2048]{3,2,0,1:T(8,128)(2,1)} %copy.27), calls=%async_computation.1 | async-start | bytes 10485760 | tf_op jit(solution)/shard_map/all_to_all | solution.py:69
  335.1 5.5 %copy-start.6 = (f32[2048]{0:T(1024)S(1)}, f32[2048]{0:T(1024)}, u32[]{:S(2)}) copy-start(f32[2048]{0:T(1024)} %param.21) | copy-start | bytes 24580
Sparse Core Ops, SparseCore 0:
  8.9 20.8 all-gather.3
  31.3 19.2 all-gather.5
  52.1 21.0 all-gather.7
where the time goes:
time: 351 us; the launch traced here: 350 us
  waiting for transfers between devices  229 us (65%)
  local copies, waits for them, and re-layouts  43.2 us (12%)
  matrix products  39.8 us (11%)
  between operations  13.3 us (4%)
  other arithmetic  12.6 us (4%)
  starting transfers between devices  12.3 us (4%)
    all_to_all x1, waiting for transfers between devices, body(): lax.all_to_all(outgoing, 'ep', split_axis=0, concat_axis=1, tiled=True)  115 us
    all_to_all x1, waiting for transfers between devices, body(): lax.all_to_all(result, 'ep', split_axis=1, concat_axis=0, tiled=True)  111 us
    dot_general x1, matrix products, expert_rows(): jnp.einsum('erf,efd->erd', hidden, w_down, preferred_element_type=jnp.flo...  16.2 us
    gather x1, local copies, waits for them, and re-layouts, body(): back_rows[position].reshape(tok_count, top_count, width).astype(jnp.float32)  12 us
    dot_general x1, matrix products, expert_rows(): jnp.einsum('erd,edf->erf', tok_rows, w_gate, preferred_element_type=jnp.f...  9.3 us
    another operation x3, other arithmetic  9.14 us
    all_to_all x1, starting transfers between devices, body(): lax.all_to_all(outgoing, 'ep', split_axis=0, concat_axis=1, tiled=True)  7.31 us
    reshape x1, local copies, waits for them, and re-layouts, body(): back_rows[position].reshape(tok_count, top_count, width).astype(jnp.float32)  7.18 us
  transfers between devices with their start and end apart: 5, of which 2 were waited for; matrix products, arithmetic and copies ran while one was open for 11% of the time, Pallas kernels for 0%

commit v1 on v0

--- a/solution.py
+++ b/solution.py
@@ -1,6 +1,10 @@
+import functools
+
 import jax
 import jax.numpy as jnp
 from jax import lax
+from jax.experimental import pallas as pl
+from jax.experimental.pallas import tpu as pltpu
 from jax.sharding import PartitionSpec as P
 
 EXPERTS = 32
@@ -74,10 +78,381 @@
     combined = routed + shared_out
     return rms_scale(combined, post_gain).astype(jnp.bfloat16)
 
+VMEM_ALL = 67043328
+MESH = pl.DeviceIdType.MESH
+AHEAD = 2
+
+
+def ring_place(ep, n):
+    half, odd = ep // 2, ep % 2
+    return half * (1 - odd) + (n - 1 - half) * odd
+
+
+def ring_member(place, n):
+    back = place // (n // 2)
+    return 2 * place * (1 - back) + (2 * (n - 1 - place) + 1) * back
+
+
+def kernel(
+    n,
+    top,
+    tok_ref,
+    meta_ref,
+    ngain_ref,
+    pgain_ref,
+    eg_hbm,
+    eu_hbm,
+    ed_hbm,
+    sg_hbm,
+    su_hbm,
+    sd_hbm,
+    out_ref,
+    wg,
+    wu,
+    wd,
+    sg,
+    su,
+    sd,
+    ag,
+    meta,
+    rs_in,
+    rs_out,
+    part,
+    shared,
+    hid,
+    cols,
+    load_sem,
+    w_send,
+    w_recv,
+    ag_send,
+    ag_recv,
+    mt_send,
+    mt_recv,
+    rs_send,
+    rs_recv,
+):
+    rows, width = tok_ref.shape
+    experts = eg_hbm.shape[0]
+    fh = eg_hbm.shape[2]
+    half = rows // 2
+    step_rows = 32
+    ep = lax.axis_index("ep")
+    tp = lax.axis_index("tp")
+    me = ring_place(ep, n)
+    right = ring_member((me + 1) % n, n)
+    left = ring_member((me + n - 1) % n, n)
+    partner = 1 - tp
+
+    barrier = pltpu.get_barrier_semaphore()
+    for where in ({"ep": right}, {"ep": left}, {"tp": partner}):
+        pl.semaphore_signal(barrier, inc=1, device_id=where, device_id_type=MESH)
+
+    loads = [
+        pltpu.make_async_copy(src, dst, load_sem.at[k])
+        for k, (src, dst) in enumerate(
+            (
+                (sg_hbm, sg),
+                (su_hbm, su),
+                (sd_hbm, sd),
+                (eg_hbm, wg.at[0]),
+                (eu_hbm, wu.at[0]),
+                (ed_hbm, wd.at[0]),
+            )
+        )
+    ]
+    for load in loads:
+        load.start()
+
+    meta[0] = meta_ref[...]
+
+    @pl.loop(0, rows // step_rows)
+    def _(r):
+        at = pl.ds(pl.multiple_of(r * step_rows, step_rows), step_rows)
+        v = tok_ref[at, :].astype(jnp.float32)
+        ag[0, at, :] = rms_scale(v, ngain_ref[...]).astype(jnp.bfloat16)
+
+    pl.semaphore_wait(barrier, 3)
+
+    def token_copy(way, s):
+        lane = pl.ds(way * half, half)
+        return pltpu.make_async_remote_copy(
+            src_ref=ag.at[s, lane],
+            dst_ref=ag.at[s + 1, lane],
+            send_sem=ag_send.at[way, s],
+            recv_sem=ag_recv.at[way, s + 1],
+            device_id={"ep": (right, left)[way]},
+            device_id_type=MESH,
+        )
+
+    def meta_copy(way, s):
+        lane = pl.ds(way * half, half)
+        return pltpu.make_async_remote_copy(
+            src_ref=meta.at[s, :, lane],
+            dst_ref=meta.at[s + 1, :, lane],
+            send_sem=mt_send.at[way, s],
+            recv_sem=mt_recv.at[way, s + 1],
+            device_id={"ep": (right, left)[way]},
+            device_id_type=MESH,
+        )
+
+    def sum_copy(way, s):
+        lane = pl.ds(way * half, half)
+        return pltpu.make_async_remote_copy(
+            src_ref=rs_out.at[s % 2, lane],
+            dst_ref=rs_in.at[s - 1, lane],
+            send_sem=rs_send.at[way, s % 2],
+            recv_sem=rs_recv.at[way, s - 1],
+            device_id={"ep": (right, left)[way]},
+            device_id_type=MESH,
+        )
+
+    for way in range(2):
+        meta_copy(way, 0).start()
+        token_copy(way, 0).start()
+
+    swaps = [
+        pltpu.make_async_remote_copy(
+            src_ref=src,
+            dst_ref=dst.at[1],
+            send_sem=w_send.at[k],
+            recv_sem=w_recv.at[k],
+            device_id={"tp": partner},
+            device_id_type=MESH,
+        )
+        for k, (src, dst) in enumerate(((eg_hbm, wg), (eu_hbm, wu), (ed_hbm, wd)))
+    ]
+    for swap in swaps:
+        swap.start()
+
+    def take(s):
+        for way in range(2):
+            meta_copy(way, s - 1).wait_recv()
+            token_copy(way, s - 1).wait_recv()
+
+            @pl.when(s < n - 1)
+            def _():
+                meta_copy(way, s).start()
+                token_copy(way, s).start()
+
+    for load in loads[:3]:
+        load.wait()
+    fs = sg.shape[1]
+    for k in range(fs // fh):
+        at = slice(k * fh, (k + 1) * fh)
+        g = jnp.dot(ag[0], sg[:, at], preferred_element_type=jnp.float32)
+        u = jnp.dot(ag[0], su[:, at], preferred_element_type=jnp.float32)
+        hid[0, :, at] = (jax.nn.silu(g) * u).astype(jnp.bfloat16)
+
+    tile = min(512, width)
+
+    @pl.loop(0, width // tile)
+    def _(j):
+        at = pl.ds(pl.multiple_of(j * tile, tile), tile)
+        shared[:, at] = jnp.dot(hid[0, :, :fs], sd[:, at], preferred_element_type=jnp.float32)
+
+    for s in range(1, min(AHEAD, n - 1) + 1):
+        take(s)
+    for load in loads[3:]:
+        load.wait()
+    for swap in swaps:
+        swap.wait_recv()
+
+    def block(slot):
+        table = meta[slot]
+        lines = []
+        for j in range(experts):
+            number = (ep * experts + j).astype(jnp.float32)
+            hit = jnp.where(table[:top] == number, table[top : 2 * top], 0.0)
+            lines.append(jnp.sum(hit, axis=0, keepdims=True))
+        lines.append(jnp.zeros((-experts % 8, rows), jnp.float32)) if experts % 8 else None
+        turned = jnp.concatenate(lines, axis=0).T
+        for j in range(experts):
+            cols[j] = jnp.broadcast_to(turned[:, j : j + 1], (rows, 128))
+
+        @pl.loop(0, experts)
+        def _(e):
+            scale = cols[e][:, :1]
+            at = pl.ds(pl.multiple_of(e * fh, fh), fh)
+            for h in range(2):
+                g = jnp.dot(ag[slot], wg[h, e], preferred_element_type=jnp.float32)
+                u = jnp.dot(ag[slot], wu[h, e], preferred_element_type=jnp.float32)
+                hid[h, :, at] = (jax.nn.silu(g) * u * scale).astype(jnp.bfloat16)
+
+        @pl.loop(0, width // tile)
+        def _(j):
+            at = pl.ds(pl.multiple_of(j * tile, tile), tile)
+            total = jnp.zeros((rows, tile), jnp.float32)
+            for h in range(2):
+                down = wd[h, :, :, at].reshape(experts * fh, tile)
+                total += jnp.dot(hid[h], down, preferred_element_type=jnp.float32)
+            part[:, at] = total
+
+    def each_rows(fn):
+        @pl.loop(0, rows // step_rows)
+        def _(r):
+            fn(pl.ds(pl.multiple_of(r * step_rows, step_rows), step_rows))
+
+    @pl.loop(1, n + 1)
+    def _(s):
+        block(s % n)
+
+        @pl.when(s + AHEAD < n)
+        def _():
+            take(s + AHEAD)
+
+        @pl.when(s > 1)
+        def _():
+            for way in range(2):
+                sum_copy(way, s - 1).wait_recv()
+
+        @pl.when(s < n)
+        def _():
+            @pl.when(s > 2)
+            def _():
+                for way in range(2):
+                    sum_copy(way, s - 2).wait_send()
+
+            @pl.when(s == 1)
+            def _():
+                def put(at):
+                    rs_out[s % 2, at, :] = part[at, :].astype(jnp.bfloat16)
+
+                each_rows(put)
+
+            @pl.when(s > 1)
+            def _():
+                def put(at):
+                    both = part[at, :] + rs_in[s - 2, at, :].astype(jnp.float32)
+                    rs_out[s % 2, at, :] = both.astype(jnp.bfloat16)
+
+                each_rows(put)
+
+            for way in range(2):
+                sum_copy(way, s).start()
+
+    def finish(at):
+        both = part[at, :] + rs_in[n - 2, at, :].astype(jnp.float32) + shared[at, :]
+        out_ref[at, :] = rms_scale(both, pgain_ref[...]).astype(jnp.bfloat16)
+
+    each_rows(finish)
+
+    for swap in swaps:
+        swap.wait_send()
+    for way in range(2):
+        for s in range(n - 1):
+            meta_copy(way, s).wait_send()
+            token_copy(way, s).wait_send()
+        for s in range(max(1, n - 2), n):
+            sum_copy(way, s).wait_send()
+
+
+def ring_shapes(n, rows, width, meta_rows, eg, ed, sg, sd):
+    bf, f32 = jnp.bfloat16, jnp.float32
+    experts, _, fh = eg.shape
+    fs = sg.shape[1]
+    return [
+        ((2,) + eg.shape, bf),
+        ((2,) + eg.shape, bf),
+        ((2,) + ed.shape, bf),
+        (sg.shape, bf),
+        (sg.shape, bf),
+        (sd.shape, bf),
+        ((n, rows, width), bf),
+        ((n, meta_rows, rows), f32),
+        ((n - 1, rows, width), bf),
+        ((2, rows, width), bf),
+        ((rows, width), f32),
+        ((rows, width), f32),
+        ((2, rows, max(experts * fh, fs)), bf),
+        ((experts, rows, 128), f32),
+    ]
+
+
+def ring_bytes(shapes):
+    total = 0
+    for shape, kind in shapes:
+        count = jnp.dtype(kind).itemsize
+        for size in shape:
+            count *= size
+        total += count
+    return total
+
+
+def ring_body(
+    n,
+    tokens,
+    norm_gain,
+    expert_ids,
+    gate_weights,
+    expert_gate,
+    expert_up,
+    expert_down,
+    shared_gate,
+    shared_up,
+    shared_down,
+    post_gain,
+):
+    rows, width = tokens.shape
+    top = expert_ids.shape[1]
+    meta_rows = -(-2 * top // 8) * 8
+    shapes = ring_shapes(n, rows, width, meta_rows, expert_gate, expert_down, shared_gate, shared_down)
+    if ring_bytes(shapes) + 4 * rows * width > VMEM_ALL - (2 << 20):
+        return body(
+            tokens,
+            norm_gain,
+            expert_ids,
+            gate_weights,
+            expert_gate,
+            expert_up,
+            expert_down,
+            shared_gate,
+            shared_up,
+            shared_down,
+            post_gain,
+        )
+    meta = jnp.concatenate([expert_ids.T.astype(jnp.float32), gate_weights.T], axis=0)
+    meta = jnp.pad(meta, ((0, meta_rows - 2 * top), (0, 0)))
+    dma = pltpu.SemaphoreType.DMA
+    vmem = pl.BlockSpec(memory_space=pltpu.VMEM)
+    hbm = pl.BlockSpec(memory_space=pl.ANY)
+    return pl.pallas_call(
+        functools.partial(kernel, n, top),
+        out_shape=jax.ShapeDtypeStruct((rows, width), jnp.bfloat16),
+        in_specs=[vmem] * 4 + [hbm] * 6,
+        out_specs=vmem,
+        scratch_shapes=[pltpu.VMEM(shape, kind) for shape, kind in shapes]
+        + [
+            dma((6,)),
+            dma((3,)),
+            dma((3,)),
+            dma((2, n)),
+            dma((2, n)),
+            dma((2, n)),
+            dma((2, n)),
+            dma((2, 2)),
+            dma((2, n)),
+        ],
+        compiler_params=pltpu.CompilerParams(
+            collective_id=0, has_side_effects=True, vmem_limit_bytes=VMEM_ALL
+        ),
+    )(
+        tokens,
+        meta,
+        norm_gain.reshape(1, width),
+        post_gain.reshape(1, width),
+        expert_gate,
+        expert_up,
+        expert_down,
+        shared_gate,
+        shared_up,
+        shared_down,
+    )
+
 
 def solution(mesh):
+    ringed = mesh.shape["tp"] == 2 and mesh.shape["ep"] % 2 == 0 and mesh.shape["ep"] > 2
     return jax.shard_map(
-        body,
+        functools.partial(ring_body, mesh.shape["ep"]) if ringed else body,
         mesh=mesh,
         in_specs=(
             P(("grp", "ep", "tp"), None),

time: 351 us -> 175 us (0.50)
  waiting for transfers between devices: 229 us -> 0 us
  Pallas kernels: 0 us -> 171 us
  local copies, waits for them, and re-layouts: 43.2 us -> 2.3 us
  matrix products: 39.8 us -> 0 us
  between operations: 13.3 us -> 0.01 us
  starting transfers between devices: 12.3 us -> 0 us
  other arithmetic: 12.6 us -> 1.98 us
    all_to_all x2 -> x0, waiting for transfers between devices: 226 us -> none  [the longest x1 115 us: body(): lax.all_to_all(outgoing, 'ep', split_axis=0, concat_axis=1, tiled=True)]
    pallas_call x0 -> x1, Pallas kernels: none -> 171 us  [ring_body(): pl.pallas_call(functools.partial(kernel, n, top), out_shape=jax.ShapeDtyp...]
    dot_general x5 -> x0, matrix products: 39.8 us -> none  [the longest x1 16.2 us: expert_rows(): jnp.einsum('erf,efd->erd', hidden, w_down, preferred_element_type=jnp.flo...]
    gather x2 -> x0, local copies, waits for them, and re-layouts: 18.2 us -> none  [the longest x1 12 us: body(): back_rows[position].reshape(tok_count, top_count, width).astype(jnp.float32)]
    reshape x2 -> x0, local copies, waits for them, and re-layouts: 12.8 us -> none  [the longest x1 7.18 us: body(): back_rows[position].reshape(tok_count, top_count, width).astype(jnp.float32)]
    all_to_all x2 -> x0, starting transfers between devices: 12.3 us -> none  [the longest x1 7.31 us: body(): lax.all_to_all(outgoing, 'ep', split_axis=0, concat_axis=1, tiled=True)]
    another operation x3 -> x0, other arithmetic: 9.14 us -> none
    all_to_all x1 -> x0, local copies, waits for them, and re-layouts: 5.72 us -> none  [body(): lax.all_to_all(outgoing, 'ep', split_axis=0, concat_axis=1, tiled=True)]
  transfers between devices with their start and end apart: 5 -> 0, of which waited for: 2 -> 0; matrix products, arithmetic and copies ran while one was open for 11% -> 0% of each run, Pallas kernels for 0% -> 0%
where the time goes in v1:
time: 175 us
  Pallas kernels  171 us (98%)
  local copies, waits for them, and re-layouts  2.3 us (1%)
  other arithmetic  1.98 us (1%)
    pallas_call x1, Pallas kernels, ring_body(): pl.pallas_call(functools.partial(kernel, n, top), out_shape=jax.ShapeDtyp...  171 us

profile of v1, /device:TPU:0, one launch (start us, length us, event | category | flops | bytes accessed | tf_op | source)
XLA Modules:
  0.0 174.8 jit_solution(1549741526391218253)
XLA Ops:
  0.0 0.7 convert_bitcast_fusion
  0.7 1.3 pad_maximum_fusion.meta_ref
  2.0 170.5 %shard_map.109 = bf16[256,2048]{1,0:T(8,128)(2,1)} custom-call(bf16[256,2048]{1,0:T(8,128)(2,1)} %tok_ref.1, f32[8,256]{1,0:T(8,128)} %pad_maximum_fusion.meta_ref, f32[1,2048]{1,0:T(1,128)} %bitcast.5, f32[1,2048]{1,0:T(1,128)} %bitcast.6, bf16[4,2048,256]{2,1,0:T(8,128)(2,1)} %eg_hbm.1, bf16[4,2048,256]{2,1,0:T(8,128)(2,1)} %eu_hbm.1, ...), custom_call_target="tpu_custom_call" | custom-call | tf_op jit(solution)/shard_map/pallas_call | solution.py:418
  172.5 2.3 %copy.13 = bf16[256,2048]{1,0:T(8,128)(2,1)} copy(bf16[256,2048]{1,0:T(8,128)(2,1)} %shard_map.109) | data formatting | bytes 2097152

commit v2 on v1

v2 whole, which is shorter than its diff:
```python
import functools

import jax
import jax.numpy as jnp
from jax import lax
from jax.experimental import pallas as pl
from jax.experimental.pallas import tpu as pltpu
from jax.sharding import PartitionSpec as P

EXPERTS = 32
CAP = 40


EPS = 1e-06


def rms_scale(inputs, gain):
    mean_sq = jnp.mean(inputs * inputs, axis=-1, keepdims=True)
    return inputs * lax.rsqrt(mean_sq + EPS) * gain


def expert_rows(tok_rows, w_gate, w_up, w_down):
    gate_act = jnp.einsum("erd,edf->erf", tok_rows, w_gate, preferred_element_type=jnp.float32)
    up_act = jnp.einsum("erd,edf->erf", tok_rows, w_up, preferred_element_type=jnp.float32)
    hidden = (jax.nn.silu(gate_act) * up_act).astype(jnp.bfloat16)
    return jnp.einsum("erf,efd->erd", hidden, w_down, preferred_element_type=jnp.float32)


def shared_branch(normed, shared_gate, shared_up, shared_down):
    shared_act = jnp.dot(normed, shared_gate, preferred_element_type=jnp.float32)
    shared_lift = jnp.dot(normed, shared_up, preferred_element_type=jnp.float32)
    shared_hidden = (jax.nn.silu(shared_act) * shared_lift).astype(jnp.bfloat16)
    return jnp.dot(shared_hidden, shared_down, preferred_element_type=jnp.float32)


def body(
    tokens,
    norm_gain,
    expert_ids,
    gate_weights,
    expert_gate,
    expert_up,
    expert_down,
    shared_gate,
    shared_up,
    shared_down,
    post_gain,
):
    tok_count = tokens.shape[0]
    top_count = expert_ids.shape[1]
    width = tokens.shape[1]
    normed = rms_scale(tokens.astype(jnp.float32), norm_gain).astype(jnp.bfloat16)
    flat_ids = expert_ids.reshape(-1)
    onehot = (flat_ids[:, None] == jnp.arange(EXPERTS, dtype=jnp.int32)[None, :]).astype(jnp.int32)
    slot_index = jnp.sum(jnp.cumsum(onehot, axis=0) * onehot, axis=1) - 1
    position = flat_ids * CAP + slot_index
    source_row = jnp.arange(tok_count * top_count, dtype=jnp.int32) // top_count
    lookup = jnp.full((EXPERTS * CAP,), tok_count, jnp.int32).at[position].set(source_row)
    padded = jnp.concatenate([normed, jnp.zeros((1, width), jnp.bfloat16)], axis=0)
    outgoing = padded[lookup].reshape(EXPERTS, 1, CAP, width)
    whole_gate, whole_up, whole_down = (
        lax.all_gather(expert_gate, "tp", axis=2, tiled=True),
        lax.all_gather(expert_up, "tp", axis=2, tiled=True),
        lax.all_gather(expert_down, "tp", axis=1, tiled=True),
    )
    arrived = lax.all_to_all(outgoing, "ep", split_axis=0, concat_axis=1, tiled=True)
    local_experts = arrived.shape[0]
    senders = arrived.shape[1]
    slots = arrived.shape[2]
    tok_rows = arrived.reshape(local_experts, senders * slots, width)
    result = expert_rows(tok_rows, whole_gate, whole_up, whole_down).astype(jnp.bfloat16)
    result = result.reshape(local_experts, senders, slots, width)
    returned = lax.all_to_all(result, "ep", split_axis=1, concat_axis=0, tiled=True)
    shared_out = shared_branch(normed, shared_gate, shared_up, shared_down)
    back_rows = returned.reshape(EXPERTS * CAP, width)
    picked = back_rows[position].reshape(tok_count, top_count, width).astype(jnp.float32)
    routed = jnp.einsum("tk,tkd->td", gate_weights, picked)
    combined = routed + shared_out
    return rms_scale(combined, post_gain).astype(jnp.bfloat16)

VMEM_ALL = 67043328
MESH = pl.DeviceIdType.MESH


TAKE, SERVE, DENSE, MERGE, WAIT = range(5)
PLANS = {
    4: (
        ("T1", "W0", "S0", "D0", "S1", "T2", "D1", "M1", "S2", "T3", "D2", "M2", "S3", "D3", "M3", "M0"),
        ("T2", "T0", "W0", "S1", "D1", "S2", "T3", "S0", "D2", "S3", "D3", "M2", "D0", "M3", "M0", "M1"),
    ),
}


def is_equal(value, k, size):
    def at_least(low):
        return (value + size - low) // size if low < size else 0

    return at_least(k) - at_least(k + 1) if k > 0 else 1 - at_least(1)


def step_of(plan, z, i, size):
    mirror = z // (size // 2)
    near = z * (1 - mirror) + (size - 1 - z) * mirror
    words = plan
    count = len(words[0])
    kind, block = 0, 0
    for k in range(count):
        here = is_equal(i, k, count)
        for r in range(len(plan)):
            both = here * is_equal(near, r, len(plan))
            kind = kind + "TSDMW".index(words[r][k][0]) * both
            block = block + int(words[r][k][1]) * both
    return kind, block * (1 - mirror) + (size - 1 - block) * mirror


def kernel(
    size,
    top,
    tok_ref,
    meta_ref,
    ngain_ref,
    pgain_ref,
    eg_hbm,
    eu_hbm,
    ed_hbm,
    sg_hbm,
    su_hbm,
    sd_hbm,
    out_ref,
    wg,
    wu,
    wd,
    sg,
    su,
    sd,
    ag,
    meta,
    y_out,
    y_in,
    yr_in,
    rs_in,
    rs_out,
    stage,
    hid,
    cols,
    tri,
    load_sem,
    w_send,
    w_recv,
    ag_send,
    ag_recv,
    mt_send,
    mt_recv,
    yd_send,
    yd_recv,
    yr_send,
    yr_recv,
    rs_send,
    rs_recv,
):
    rows, width = tok_ref.shape
    experts = eg_hbm.shape[0]
    fh = eg_hbm.shape[2]
    slots = experts * CAP
    step_rows = 32
    tile = min(512, width)
    pieces = width // tile
    last = size - 1
    bf, f32 = jnp.bfloat16, jnp.float32
    ep = lax.axis_index("ep")
    z, y = ep // 2, ep % 2
    pair = z * 2 + 1 - y
    partner = 1 - lax.axis_index("tp")
    plan = PLANS[size]

    barrier = pltpu.get_barrier_semaphore()

    def greet(where):
        pl.semaphore_signal(barrier, inc=1, device_id=where, device_id_type=MESH)

    @pl.when(z < last)
    def _():
        greet({"ep": (z + 1) * 2 + y})

    @pl.when(z > 0)
    def _():
        greet({"ep": (z - 1) * 2 + y})

    greet({"ep": pair})
    greet({"tp": partner})

    loads = [
        pltpu.make_async_copy(src, dst, load_sem.at[k])
        for k, (src, dst) in enumerate(
            (
                (sg_hbm, sg),
                (su_hbm, su),
                (sd_hbm, sd),
                (eg_hbm, wg.at[0]),
                (eu_hbm, wu.at[0]),
                (ed_hbm, wd.at[0]),
            )
        )
    ]
    for load in loads:
        load.start()

    meta[z] = meta_ref[...]
    before = lax.broadcasted_iota(jnp.int32, (rows, rows), 0) < lax.broadcasted_iota(jnp.int32, (rows, rows), 1)
    tri[...] = jnp.where(before, 1.0, 0.0).astype(bf)

    @pl.loop(0, rows // step_rows)
    def _(r):
        at = pl.ds(pl.multiple_of(r * step_rows, step_rows), step_rows)
        v = tok_ref[at, :].astype(f32)
        ag[z, at, :] = rms_scale(v, ngain_ref[...]).astype(bf)

    pl.semaphore_wait(barrier, 2 + (z + last) // size + (last - z + last) // size)

    def piece(q):
        return pl.ds(q * tile, tile)

    def remote(src, dst, send, recv, where):
        return pltpu.make_async_remote_copy(
            src_ref=src, dst_ref=dst, send_sem=send, recv_sem=recv, device_id=where, device_id_type=MESH
        )

    def token_copy(b, q, zt, slot):
        ref = ag.at[b, :, piece(q)]
        return remote(ref, ref, ag_send.at[slot, q], ag_recv.at[b, q], {"ep": zt * 2 + y})

    def meta_copy(b, zt, slot):
        return remote(meta.at[b], meta.at[b], mt_send.at[slot], mt_recv.at[b], {"ep": zt * 2 + y})

    def row_copy(b, q):
        at = piece(q)
        return remote(y_out.at[b, :, at], y_in.at[b, :, at], yd_send.at[b, q], yd_recv.at[b, q], {"ep": pair})

    def back_copy(b, q):
        at = piece(q)
        return remote(y_in.at[b, :, at], yr_in.at[b, :, at], yr_send.at[b, q], yr_recv.at[b, q], {"ep": pair})

    def sum_copy(b, q, zt, slot):
        at = piece(q)
        return remote(
            rs_out.at[b, :, at], rs_in.at[slot, :, at], rs_send.at[b, q], rs_recv.at[slot, q], {"ep": zt * 2 + y}
        )

    def own_sends(act):
        @pl.when(z < last)
        def _():
            act(meta_copy(z, z + 1, z))

        @pl.when(z > 0)
        def _():
            act(meta_copy(z, z - 1, size))

        for q in range(pieces):

            @pl.when(z < last)
            def _():
                act(token_copy(z, q, z + 1, z))

            @pl.when(z > 0)
            def _():
                act(token_copy(z, q, z - 1, size))

    own_sends(lambda copy: copy.start())

    def onward(b, fn):
        @pl.when((b < z) & (z < last))
        def _():
            fn(z + 1)

        @pl.when((b > z) & (z > 0))
        def _():
            fn(z - 1)

    def targets(b, number_of):
        seen = meta[b]
        hits, weights = [], []
        for j in range(experts):
            number = (number_of * experts + j).astype(f32)
            same = seen[:top] == number
            hits.append(jnp.sum(jnp.where(same, 1.0, 0.0), axis=0, keepdims=True))
            weights.append(jnp.sum(jnp.where(same, seen[top : 2 * top], 0.0), axis=0, keepdims=True))
        blank = -experts % 8
        if blank:
            hits.append(jnp.zeros((blank, rows), f32))
            weights.append(jnp.zeros((blank, rows), f32))
        return jnp.concatenate(hits, axis=0), jnp.concatenate(weights, axis=0)

    def places(hits):
        rank = jnp.dot(hits.astype(bf), tri[...], preferred_element_type=f32)
        first = lax.broadcasted_iota(jnp.int32, hits.shape, 0).astype(f32) * CAP
        return jnp.where(hits > 0.0, rank + first, -1.0)

    def dispatch(b):
        hits, _ = targets(b, pair)
        spot = places(hits)
        line = lax.broadcasted_iota(jnp.int32, (slots, rows), 0).astype(f32)
        pick = jnp.zeros((slots, rows), f32)
        for j in range(experts):
            pick = jnp.where(line == spot[j : j + 1], 1.0, pick)
        pick = pick.astype(bf)
        for q in range(pieces):
            at = piece(q)
            y_out[b, :, at] = jnp.dot(pick, ag[b, :, at], preferred_element_type=f32).astype(bf)
            row_copy(b, q).start()

    def take(b):
        meta_copy(b, z, z).wait_recv()
        onward(b, lambda zt: meta_copy(b, zt, b).start())
        for q in range(pieces):
            token_copy(b, q, z, z).wait_recv()
            onward(b, lambda zt: token_copy(b, q, zt, b).start())
        dispatch(b)

    def hidden_of(x_ref, scale_of, count):
        @pl.loop(0, experts)
        def _(e):
            scale = scale_of(e)
            at = pl.ds(pl.multiple_of(e * fh, fh), fh)
            for h in range(2):
                g = jnp.dot(x_ref[...], wg[h, e], preferred_element_type=f32)
                u = jnp.dot(x_ref[...], wu[h, e], preferred_element_type=f32)
                hid[h, :count, at] = (jax.nn.silu(g) * u * scale).astype(bf)

    def down_of(count, q):
        total = jnp.zeros((count, tile), f32)
        for h in range(2):
            down = wd[h, :, :, piece(q)].reshape(experts * fh, tile)
            total += jnp.dot(hid[h, :count, : experts * fh], down, preferred_element_type=f32)
        return total

    def serve(b):
        for q in range(pieces):
            row_copy(b, q).wait_recv()
        line = lax.broadcasted_iota(jnp.int32, (slots, fh), 0)
        hidden_of(
            y_in.at[b],
            lambda e: jnp.where((line >= e * CAP) & (line < (e + 1) * CAP), 1.0, 0.0),
            slots,
        )
        for q in range(pieces):
            y_in[b, :, piece(q)] = down_of(slots, q).astype(bf)
            back_copy(b, q).start()

    def place_of(b):
        apart = ((b - z) * (b - z) + size * size - 1) // (size * size)
        return 2 - apart * (2 - b % 2)

    def dense(b):
        _, weights = targets(b, ep)
        turned = weights.T
        for j in range(experts):
            cols[j] = jnp.broadcast_to(turned[:, j : j + 1], (rows, 128))
        hidden_of(ag.at[b], lambda e: cols[e][:, :1], rows)
        for q in range(pieces):
            total = down_of(rows, q)

            @pl.when(b == z)
            def _():
                stage[2, :, piece(q)] += total

            @pl.when(b != z)
            def _():
                stage[b % 2, :, piece(q)] = total

    def merge(b):
        hits, weights = targets(b, pair)
        spot = places(hits).T
        turned = weights.T
        lane = lax.broadcasted_iota(jnp.int32, (rows, slots), 1).astype(f32)
        mix = jnp.zeros((rows, slots), f32)
        for j in range(experts):
            mix = jnp.where(lane == spot[:, j : j + 1], turned[:, j : j + 1], mix)
        high = mix.astype(bf)
        low = (mix - high.astype(f32)).astype(bf)
        own = b == z
        here = place_of(b)

        for q in range(pieces):
            at = piece(q)
            back_copy(b, q).wait_recv()
            came = yr_in[b, :, at]
            stage[here, :, at] += jnp.dot(high, came, preferred_element_type=f32) + jnp.dot(
                low, came, preferred_element_type=f32
            )

            @pl.when(((b >= z) & (z > 0)) | ((b < z) & (z < last)))
            def _():
                sum_copy(b, q, z, b).wait_recv()
                stage[here, :, at] += rs_in[b, :, at].astype(f32)

            @pl.when(own & (z < last))
            def _():
                sum_copy(b, q, z, size).wait_recv()
                stage[here, :, at] += rs_in[size, :, at].astype(f32)

            @pl.when(jnp.logical_not(own))
            def _():
                rs_out[b, :, at] = stage[here, :, at].astype(bf)

            @pl.when(b > z)
            def _():
                sum_copy(b, q, z + 1, b).start()

            @pl.when(b < z - 1)
            def _():
                sum_copy(b, q, z - 1, b).start()

            @pl.when(b == z - 1)
            def _():
                sum_copy(b, q, z - 1, size).start()

    swaps = [
        remote(src, dst.at[1], w_send.at[k], w_recv.at[k], {"tp": partner})
        for k, (src, dst) in enumerate(((eg_hbm, wg), (eu_hbm, wu), (ed_hbm, wd)))
    ]
    dispatch(z)
    for swap in swaps:
        swap.start()

    for load in loads[:3]:
        load.wait()
    fs = sg.shape[1]
    for k in range(fs // fh):
        at = slice(k * fh, (k + 1) * fh)
        g = jnp.dot(ag[z], sg[:, at], preferred_element_type=f32)
        u = jnp.dot(ag[z], su[:, at], preferred_element_type=f32)
        hid[0, :, at] = (jax.nn.silu(g) * u).astype(bf)

    @pl.loop(0, pieces)
    def _(j):
        at = pl.ds(pl.multiple_of(j * tile, tile), tile)
        stage[2, :, at] = jnp.dot(hid[0, :, :fs], sd[:, at], preferred_element_type=f32)

    def weights_in(b):
        for load in loads[3:]:
            load.wait()
        for swap in swaps:
            swap.wait_recv()

    @pl.loop(0, len(plan[0]))
    def _(i):
        kind, b = step_of(plan, z, i, size)
        for number, fn in ((TAKE, take), (SERVE, serve), (DENSE, dense), (MERGE, merge), (WAIT, weights_in)):

            @pl.when(kind == number)
            def _():
                fn(b)

    @pl.loop(0, rows // step_rows)
    def _(r):
        at = pl.ds(pl.multiple_of(r * step_rows, step_rows), step_rows)
        out_ref[at, :] = rms_scale(stage[2, at, :], pgain_ref[...]).astype(bf)

    for swap in swaps:
        swap.wait_send()
    own_sends(lambda copy: copy.wait_send())

    @pl.loop(0, size)
    def _(b):
        onward(b, lambda zt: meta_copy(b, zt, b).wait_send())
        for q in range(pieces):
            onward(b, lambda zt: token_copy(b, q, zt, b).wait_send())
            row_copy(b, q).wait_send()
            back_copy(b, q).wait_send()

            @pl.when(b > z)
            def _():
                sum_copy(b, q, z, b).wait_send()

            @pl.when(b < z)
            def _():
                sum_copy(b, q, z, b).wait_send()


def ring_shapes(n, rows, width, meta_rows, eg, ed, sg, sd):
    bf, f32 = jnp.bfloat16, jnp.float32
    experts, _, fh = eg.shape
    fs = sg.shape[1]
    size = n // 2
    slots = experts * CAP
    return [
        ((2,) + eg.shape, bf),
        ((2,) + eg.shape, bf),
        ((2,) + ed.shape, bf),
        (sg.shape, bf),
        (sg.shape, bf),
        (sd.shape, bf),
        ((size, rows, width), bf),
        ((size, meta_rows, rows), f32),
        ((size, slots, width), bf),
        ((size, slots, width), bf),
        ((size, slots, width), bf),
        ((size + 1, rows, width), bf),
        ((size, rows, width), bf),
        ((3, rows, width), f32),
        ((2, rows, max(experts * fh, fs)), bf),
        ((experts, rows, 128), f32),
        ((rows, rows), bf),
    ]


def ring_bytes(shapes):
    total = 0
    for shape, kind in shapes:
        count = jnp.dtype(kind).itemsize
        for size in shape:
            count *= size
        total += count
    return total


def ring_body(
    n,
    tokens,
    norm_gain,
    expert_ids,
    gate_weights,
    expert_gate,
    expert_up,
    expert_down,
    shared_gate,
    shared_up,
    shared_down,
    post_gain,
):
    rows, width = tokens.shape
    top = expert_ids.shape[1]
    meta_rows = -(-2 * top // 8) * 8
    shapes = ring_shapes(n, rows, width, meta_rows, expert_gate, expert_down, shared_gate, shared_down)
    if ring_bytes(shapes) + 4 * rows * width > VMEM_ALL - (2 << 20):
        return body(
            tokens,
            norm_gain,
            expert_ids,
            gate_weights,
            expert_gate,
            expert_up,
            expert_down,
            shared_gate,
            shared_up,
            shared_down,
            post_gain,
        )
    meta = jnp.concatenate([expert_ids.T.astype(jnp.float32), gate_weights.T], axis=0)
    meta = jnp.pad(meta, ((0, meta_rows - 2 * top), (0, 0)))
    dma = pltpu.SemaphoreType.DMA
    size = n // 2
    pieces = width // min(512, width)
    vmem = pl.BlockSpec(memory_space=pltpu.VMEM)
    hbm = pl.BlockSpec(memory_space=pl.ANY)
    return pl.pallas_call(
        functools.partial(kernel, size, top),
        out_shape=jax.ShapeDtypeStruct((rows, width), jnp.bfloat16),
        in_specs=[vmem] * 4 + [hbm] * 6,
        out_specs=vmem,
        scratch_shapes=[pltpu.VMEM(shape, kind) for shape, kind in shapes]
        + [
            dma((6,)),
            dma((3,)),
            dma((3,)),
            dma((size + 1, pieces)),
            dma((size, pieces)),
            dma((size + 1,)),
            dma((size,)),
            dma((size, pieces)),
            dma((size, pieces)),
            dma((size, pieces)),
            dma((size, pieces)),
            dma((size, pieces)),
            dma((size + 1, pieces)),
        ],
        compiler_params=pltpu.CompilerParams(
            collective_id=0, has_side_effects=True, vmem_limit_bytes=VMEM_ALL
        ),
    )(
        tokens,
        meta,
        norm_gain.reshape(1, width),
        post_gain.reshape(1, width),
        expert_gate,
        expert_up,
        expert_down,
        shared_gate,
        shared_up,
        shared_down,
    )


def solution(mesh):
    ringed = mesh.shape["tp"] == 2 and mesh.shape["ep"] % 2 == 0 and mesh.shape["ep"] // 2 in PLANS
    return jax.shard_map(
        functools.partial(ring_body, mesh.shape["ep"]) if ringed else body,
        mesh=mesh,
        in_specs=(
            P(("grp", "ep", "tp"), None),
            P(),
            P(("grp", "ep", "tp"), None),
            P(("grp", "ep", "tp"), None),
            P("ep", None, "tp"),
            P("ep", None, "tp"),
            P("ep", "tp", None),
            P(),
            P(),
            P(),
            P(),
        ),
        out_specs=P(("grp", "ep", "tp"), None),
        check_vma=False,
    )
```

time: 175 us -> 184 us (1.051)
  Pallas kernels: 171 us -> 179 us
    pallas_call x1, Pallas kernels: 171 us -> 179 us  [ring_body(): pl.pallas_call(functools.partial(kernel, size, top), out_shape=jax.ShapeD...]
where the time goes in v2:
time: 184 us; the launch traced here: 183 us
  Pallas kernels  179 us (97%)
  local copies, waits for them, and re-layouts  2.3 us (1%)
  other arithmetic  1.98 us (1%)
    pallas_call x1, Pallas kernels, ring_body(): pl.pallas_call(functools.partial(kernel, size, top), out_shape=jax.ShapeD...  179 us

profile of v2, /device:TPU:0, one launch (start us, length us, event | category | flops | bytes accessed | tf_op | source)
XLA Modules:
  0.0 183.4 jit_solution(236721876240256941)
XLA Ops:
  0.0 0.7 convert_bitcast_fusion
  0.7 1.3 pad_maximum_fusion.meta_ref
  2.0 179.1 %shard_map.109 = bf16[256,2048]{1,0:T(8,128)(2,1)} custom-call(bf16[256,2048]{1,0:T(8,128)(2,1)} %tok_ref.1, f32[8,256]{1,0:T(8,128)} %pad_maximum_fusion.meta_ref, f32[1,2048]{1,0:T(1,128)} %bitcast.5, f32[1,2048]{1,0:T(1,128)} %bitcast.6, bf16[4,2048,256]{2,1,0:T(8,128)(2,1)} %eg_hbm.1, bf16[4,2048,256]{2,1,0:T(8,128)(2,1)} %eu_hbm.1, ...), custom_call_target="tpu_custom_call" | custom-call | tf_op jit(solution)/shard_map/pallas_call | solution.py:556
  181.1 2.3 %copy.13 = bf16[256,2048]{1,0:T(8,128)(2,1)} copy(bf16[256,2048]{1,0:T(8,128)(2,1)} %shard_map.109) | data formatting | bytes 2097152

commit v3 on v2

--- a/solution.py
+++ b/solution.py
@@ -85,8 +85,8 @@
 TAKE, SERVE, DENSE, MERGE, WAIT = range(5)
 PLANS = {
     4: (
-        ("T1", "W0", "S0", "D0", "S1", "T2", "D1", "M1", "S2", "T3", "D2", "M2", "S3", "D3", "M3", "M0"),
-        ("T2", "T0", "W0", "S1", "D1", "S2", "T3", "S0", "D2", "S3", "D3", "M2", "D0", "M3", "M0", "M1"),
+        ("T1", "W0", "S0", "D0", "T2", "D2", "T3", "D3", "S3", "S2", "S1", "M3", "D1", "M2", "M1", "M0"),
+        ("T2", "T0", "W0", "D1", "T3", "S1", "D3", "S3", "S0", "D0", "S2", "M3", "M0", "D2", "M2", "M1"),
     ),
 }
 

time: 184 us -> 182 us (0.989)
  Pallas kernels: 179 us -> 177 us
    pallas_call x1, Pallas kernels: 179 us -> 177 us  [ring_body(): pl.pallas_call(functools.partial(kernel, size, top), out_shape=jax.ShapeD...]
where the time goes in v3:
time: 182 us; the launch traced here: 181 us
  Pallas kernels  177 us (97%)
  local copies, waits for them, and re-layouts  2.3 us (1%)
  other arithmetic  1.98 us (1%)
    pallas_call x1, Pallas kernels, ring_body(): pl.pallas_call(functools.partial(kernel, size, top), out_shape=jax.ShapeD...  177 us

profile of v3, /device:TPU:0, one launch (start us, length us, event | category | flops | bytes accessed | tf_op | source)
XLA Modules:
  0.0 180.8 jit_solution(1251950406518144648)
XLA Ops:
  0.0 0.7 convert_bitcast_fusion
  0.7 1.3 pad_maximum_fusion.meta_ref
  2.0 176.5 %shard_map.109 = bf16[256,2048]{1,0:T(8,128)(2,1)} custom-call(bf16[256,2048]{1,0:T(8,128)(2,1)} %tok_ref.1, f32[8,256]{1,0:T(8,128)} %pad_maximum_fusion.meta_ref, f32[1,2048]{1,0:T(1,128)} %bitcast.5, f32[1,2048]{1,0:T(1,128)} %bitcast.6, bf16[4,2048,256]{2,1,0:T(8,128)(2,1)} %eg_hbm.1, bf16[4,2048,256]{2,1,0:T(8,128)(2,1)} %eu_hbm.1, ...), custom_call_target="tpu_custom_call" | custom-call | tf_op jit(solution)/shard_map/pallas_call | solution.py:556
  178.5 2.3 %copy.13 = bf16[256,2048]{1,0:T(8,128)(2,1)} copy(bf16[256,2048]{1,0:T(8,128)(2,1)} %shard_map.109) | data formatting | bytes 2097152
